TPU v7x, 512 devices: a whole 4x8x8 slice. The times are simulated.
512 devices in a mesh: sp: 32 (over z, x), tp: 16 (over y, core).
Axes of the slice: x: 4, y: 8, z: 8, core: 2. Of those that a mesh axis runs over, the one named last changes fastest.
Arguments:
- skip_stream_entering: bfloat16 [4096, 2048], P('sp', 'tp'), may hold values from -24 to 24
- unfiltered_channel_feed: bfloat16 [4096, 2048], P('sp', 'tp'), may hold values from -6 to 6
- unfiltered_state_entry: bfloat16 [4096, 2048], P('sp', 'tp'), may hold values from -6 to 6
- unfiltered_state_exit: bfloat16 [4096, 2048], P('sp', 'tp'), may hold values from -6 to 6
- final_valve_preactivation: bfloat16 [4096, 2048], P('sp', 'tp'), may hold values from -6 to 6
- increment_preactivation: float32 [2, 32, 4096], P(None, 'tp', 'sp'), may hold values from -8 to 8
- summed_attenuation_both_ways: float32 [2, 32, 4096], P(None, 'tp', 'sp'), may hold values from -0.7 to 0, as said below
- channel_fading_speed: float32 [2, 32], P(None, 'tp'), may hold values from 4.8828125e-05 to 0.03, as said below
- channel_feed_filter: float32 [5, 2048], P(None, 'tp'), may hold values from -2.5 to 2.5
- state_entry_filter: float32 [5, 2048], P(None, 'tp'), may hold values from -2.5 to 2.5
- state_exit_filter: float32 [5, 2048], P(None, 'tp'), may hold values from -2.5 to 2.5
- clustered_rescale_factor: float32 [2048], P('tp'), may hold values from 0.1 to 1.9
- final_projection_weights: bfloat16 [2048, 2048], P(None, 'tp'), may hold values from -0.125 to 0.125
- specialist_rescale_factor: float32 [2048], replicated, may hold values from 0.1 to 1.9
- item_specialist_couple: int32 [4096, 2], P('sp'), may hold values from 0 to 31, all different within a row; in each aligned block of 128 rows (0 to 127, 128 to 255, ...) at most 16 rows name the same one
- selected_cluster_likelihood: float32 [4096], P('sp'), may hold values from 0.3 to 1
- selected_twin_scores_raw: float32 [4096, 2], P('sp'), may hold values from -6 to 6
- specialist_gating_weights: bfloat16 [32, 2048, 4096], P('sp', None, 'tp'), may hold values from -0.125 to 0.125
- specialist_raising_weights: bfloat16 [32, 2048, 4096], P('sp', None, 'tp'), may hold values from -0.125 to 0.125
- specialist_lowering_weights: bfloat16 [32, 4096, 2048], P('sp', 'tp'), may hold values from -0.09375 to 0.09375
Outputs:
- layer_out: bfloat16 [4096, 2048], P('sp', 'tp')
Inputs may be any that keep to these rules, and one draw needn't show every extreme that they name: For every head, dt times channel_fading_speed at the rate of the draw sets how far a state is carried; summed_attenuation_both_ways holds a few sharp losses of state. `summed_attenuation_both_ways`: mostly zero. `item_specialist_couple`: the two experts of a row differ. Among the rows of one index of sp (aligned blocks of 128 rows) no expert is named by more than 16 rows, a bound that some expert reaches in some blocks.
All inputs are finite; a program needn't handle non-finite values.
Results may differ from a plain program's by a relative error of at most 0.0095.
Values may be sent and summed in bfloat16 or wider, within the bound.
No kernel may reach another device: no remote copies, remote signals or barrier semaphores. Data moves between devices by JAX's collectives and lax.ppermute only.
A program may use at most 64 MiB of HBM per device.

v0:
```python
import jax
import jax.numpy as jnp
from jax import lax
from jax.sharding import Mesh
from jax.sharding import PartitionSpec as P

D = 2048
HD = 64
NS = 128
CONV = 5
SP = ("sp_0", "sp_1")
HIGHEST = lax.Precision.HIGHEST
group_eps = 1e-05
stream_eps = 1e-06


def extended(cells, sides, width):
    for axis, dim in sides:
        count = lax.axis_size(axis)
        ends = count - 1
        head = lax.slice_in_dim(cells, 0, width, axis=dim)
        tail = lax.slice_in_dim(cells, cells.shape[dim] - width, cells.shape[dim], axis=dim)
        cells = jnp.concatenate(
            [
                lax.ppermute(tail, axis, [(i, (i + 1) % count) for i in range(ends)]),
                cells,
                lax.ppermute(head, axis, [((i + 1) % count, i) for i in range(ends)]),
            ],
            axis=dim,
        )
    return cells


def filled_with(shard, identity):
    return jax.tree.map(
        lambda a, e: jnp.broadcast_to(jnp.asarray(e, a.dtype), a.shape), shard, identity
    )


def all_in_one(shard, axis):
    leaves = jax.tree.leaves(shard)
    sequence = sorted(range(len(leaves)), key=lambda k: -leaves[k].size)
    width = (1, *leaves[sequence[0]].shape)[-1]
    lines = [
        jnp.pad(leaves[k].reshape(-1), (0, -leaves[k].size % width)).reshape(-1, width)
        for k in sequence
    ]
    both, at, found = (lax.all_gather(jnp.concatenate(lines), axis), 0, {})
    for k, line in zip(sequence, lines):
        share = both[:, at : at + len(line)].reshape(len(both), -1)
        found[k] = share[:, : leaves[k].size].reshape(-1, *leaves[k].shape)
        at += len(line)
    numbers = iter(range(len(leaves)))
    return jax.tree.map(lambda _: found[next(numbers)], shard)


def carried_in(shard, axes, combine, identity, reverse):
    before = start = filled_with(shard, identity)
    so_far = shard
    for axis in reversed(axes):
        peers, mine = (lax.axis_size(axis), lax.axis_index(axis))
        pieces = all_in_one(
            jax.tree.map(
                lambda part, kind: part.astype(kind), so_far, (jnp.bfloat16, jnp.bfloat16)
            ),
            axis,
        )
        inside, so_far = (start, start)
        for k in reversed(range(peers)) if reverse else range(peers):
            passed = k > mine if reverse else k < mine
            so_far = combine(
                so_far, jax.tree.map(lambda part, own: part[k].astype(own.dtype), pieces, shard)
            )
            inside = jax.tree.map(lambda new, old: jnp.where(passed, new, old), so_far, inside)
        before = combine(inside, before)
    return before


def in_blocks(shard, dim, peers):
    shape = shard.shape
    parts = shard.reshape(*shape[:dim], peers, shape[dim] // peers, *shape[dim + 1 :])
    return jnp.moveaxis(parts, dim, 0)


def sum_at_owner(shard, axis, dim):
    peers = lax.axis_size(axis)
    parts = lax.all_to_all(in_blocks(shard, dim, peers), axis, 0, 0, tiled=True)
    return jnp.sum(parts.astype(jnp.float32), axis=0)


def block_parts(x_short, b_short, c_short, step_f, step_b, log_f, log_b):
    head_count = x_short.shape[1]
    group_count = b_short.shape[1]
    per_group = head_count // group_count
    length = x_short.shape[0]
    group_scores = jnp.einsum("tgn,sgn->gts", c_short, b_short, preferred_element_type=jnp.float32)
    x_block = x_short.astype(jnp.float32)
    b_block = b_short.astype(jnp.float32)
    c_block = c_short.astype(jnp.float32)
    scores = jnp.repeat(group_scores, per_group, axis=0)
    b_head = jnp.repeat(b_block, per_group, axis=1)
    c_head = jnp.repeat(c_block, per_group, axis=1)
    forward = jnp.cumsum(log_f, axis=1)
    backward = jnp.flip(jnp.cumsum(jnp.flip(log_b, 1), axis=1), 1)
    row_index = lax.broadcasted_iota(jnp.int32, (length, length), 0)
    col_index = lax.broadcasted_iota(jnp.int32, (length, length), 1)
    lower_mask = (col_index <= row_index)[None]
    upper_mask = (col_index >= row_index)[None]
    decay_fwd = jnp.where(
        lower_mask, jnp.exp(jnp.minimum(forward[:, :, None] - forward[:, None, :], 0.0)), 0.0
    )
    decay_bwd = jnp.where(
        upper_mask, jnp.exp(jnp.minimum(backward[:, :, None] - backward[:, None, :], 0.0)), 0.0
    )
    mixing = scores * (decay_fwd * step_f[:, None, :] + decay_bwd * step_b[:, None, :])
    within = jnp.einsum("hts,shp->thp", mixing, x_block, precision=HIGHEST)
    weight_fwd = jnp.exp(forward[:, -1:] - forward) * step_f
    weight_bwd = jnp.exp(backward[:, :1] - backward) * step_b
    state_fwd = jnp.einsum("hs,shp,shn->hpn", weight_fwd, x_block, b_head, precision=HIGHEST)
    state_bwd = jnp.einsum("hs,shp,shn->hpn", weight_bwd, x_block, b_head, precision=HIGHEST)
    return (
        within,
        state_fwd,
        state_bwd,
        forward[:, -1],
        backward[:, 0],
        jnp.exp(forward),
        jnp.exp(backward),
        c_head,
    )


def read_state(c_head, factor, state):
    return (
        jnp.einsum("thn,hpn->thp", c_head, state, precision=HIGHEST)
        * jnp.transpose(factor)[:, :, None]
    )


def compose(earlier, later):
    return (earlier[0] + later[0], earlier[1] * jnp.exp(later[0])[:, None, None] + later[1])


def body(
    skip_stream_entering,
    unfiltered_channel_feed,
    unfiltered_state_entry,
    unfiltered_state_exit,
    final_valve_preactivation,
    increment_preactivation,
    summed_attenuation_both_ways,
    channel_fading_speed,
    channel_feed_filter,
    state_entry_filter,
    state_exit_filter,
    clustered_rescale_factor,
    final_projection_weights,
    specialist_rescale_factor,
    item_specialist_couple,
    selected_cluster_likelihood,
    selected_twin_scores_raw,
    specialist_gating_weights,
    specialist_raising_weights,
    specialist_lowering_weights,
):
    tokens_here = skip_stream_entering.shape[0]
    heads_here = increment_preactivation.shape[1]
    x_width = unfiltered_channel_feed.shape[1]
    b_width = unfiltered_state_entry.shape[1]
    groups_here = b_width // NS
    joined = jnp.concatenate(
        [unfiltered_channel_feed, unfiltered_state_entry, unfiltered_state_exit], axis=1
    )
    padded = extended(joined, ((SP, 0),), CONV // 2)
    kernel = jnp.concatenate([channel_feed_filter, state_entry_filter, state_exit_filter], axis=1)
    summed = jnp.zeros(joined.shape, jnp.float32)
    for offset in range(CONV):
        summed = summed + kernel[offset] * padded[offset : offset + tokens_here].astype(jnp.float32)
    conv_out = jax.nn.silu(summed).astype(jnp.bfloat16)
    x_conv = conv_out[:, :x_width].reshape(tokens_here, heads_here, HD)
    b_conv = conv_out[:, x_width : x_width + b_width].reshape(tokens_here, groups_here, NS)
    c_conv = conv_out[:, x_width + b_width :].reshape(tokens_here, groups_here, NS)
    whole_increment_list = jax.nn.softplus(increment_preactivation)
    whole_attenuation_list = (
        -whole_increment_list * channel_fading_speed[:, :, None] + summed_attenuation_both_ways
    )
    within, state_fwd, state_bwd, total_fwd, total_bwd, factor_fwd, factor_bwd, c_head = (
        block_parts(
            x_conv,
            b_conv,
            c_conv,
            whole_increment_list[0],
            whole_increment_list[1],
            whole_attenuation_list[0],
            whole_attenuation_list[1],
        )
    )
    empty = (jnp.zeros_like(total_fwd), jnp.zeros_like(state_fwd))
    incoming_fwd = carried_in((total_fwd, state_fwd), SP, compose, empty, False)[1]
    incoming_bwd = carried_in((total_bwd, state_bwd), SP, compose, empty, True)[1]
    mixer_out = (
        within
        + read_state(c_head, factor_fwd, incoming_fwd)
        + read_state(c_head, factor_bwd, incoming_bwd)
    )
    gated = mixer_out.reshape(tokens_here, x_width) * jax.nn.silu(
        final_valve_preactivation.astype(jnp.float32)
    )
    grouped = gated.reshape(tokens_here, groups_here, -1)
    grouped = grouped * lax.rsqrt(jnp.mean(grouped * grouped, axis=-1, keepdims=True) + group_eps)
    mixed = (grouped.reshape(tokens_here, x_width) * clustered_rescale_factor).astype(jnp.bfloat16)
    projected = jnp.dot(
        lax.all_gather(mixed, "tp", axis=1, tiled=True),
        final_projection_weights,
        preferred_element_type=jnp.float32,
    )
    stream = (skip_stream_entering.astype(jnp.float32) + projected).astype(jnp.bfloat16)
    stream_f = stream.astype(jnp.float32)
    col_count = skip_stream_entering.shape[1]
    whole_rows = lax.all_gather(stream, "tp", axis=1, tiled=True).astype(jnp.float32)
    normal_rows = (
        whole_rows
        * lax.rsqrt(jnp.mean(whole_rows * whole_rows, axis=-1, keepdims=True) + stream_eps)
        * specialist_rescale_factor
    ).astype(jnp.bfloat16)
    expert_total = lax.axis_size(SP)
    capacity = 4 * tokens_here // expert_total
    flat_ids = item_specialist_couple.reshape(-1)
    assignments = flat_ids.shape[0]
    expert_iota = lax.broadcasted_iota(jnp.int32, (assignments, expert_total), 1)
    one_hot = (flat_ids[:, None] == expert_iota).astype(jnp.int32)
    ranking = jnp.sum((jnp.cumsum(one_hot, axis=0) - 1) * one_hot, axis=1)
    slot_index = flat_ids * capacity + ranking
    slot_iota = lax.broadcasted_iota(jnp.int32, (expert_total * capacity, assignments), 0)
    selector = (slot_index[None, :] == slot_iota).astype(jnp.bfloat16)
    selector = jnp.sum(selector.reshape(expert_total * capacity, tokens_here, -1), axis=2)
    weight_gate = specialist_gating_weights[0]
    weight_up = specialist_raising_weights[0]
    weight_down = specialist_lowering_weights[0]
    outgoing = jnp.dot(selector, normal_rows, preferred_element_type=jnp.float32).astype(
        jnp.bfloat16
    )
    outgoing = outgoing.reshape(expert_total, capacity, D)
    arrived = lax.all_to_all(outgoing, SP, split_axis=0, concat_axis=0, tiled=True)
    sources = arrived.shape[0]
    slot_count = arrived.shape[1]
    rows = arrived.reshape(sources * slot_count, arrived.shape[2])
    gate = jnp.dot(rows, weight_gate, preferred_element_type=jnp.float32)
    upward = jnp.dot(rows, weight_up, preferred_element_type=jnp.float32)
    hidden = (jax.nn.silu(gate) * upward).astype(jnp.bfloat16)
    partial_out = jnp.dot(hidden, weight_down, preferred_element_type=jnp.float32).astype(
        jnp.bfloat16
    )
    partial_out = partial_out.reshape(sources, slot_count, partial_out.shape[1])
    expert_cols = sum_at_owner(partial_out, "tp", 2).astype(jnp.bfloat16)
    returned = lax.all_to_all(expert_cols, SP, split_axis=0, concat_axis=0, tiled=True)
    flat_back = returned.reshape(expert_total * capacity, col_count)
    picked = (
        jnp.take(flat_back, slot_index, axis=0)
        .astype(jnp.float32)
        .reshape(tokens_here, -1, col_count)
    )
    first = jax.nn.sigmoid(selected_twin_scores_raw[:, 0] - selected_twin_scores_raw[:, 1])
    route_weight = selected_cluster_likelihood[:, None] * jnp.stack([first, 1.0 - first], axis=1)
    experts_sum = jnp.sum(route_weight[:, :, None] * picked, axis=1)
    return (stream_f + experts_sum).astype(jnp.bfloat16)


def solution(mesh):
    torus = Mesh(mesh.devices.reshape(8, 4, mesh.shape["tp"]), ("sp_0", "sp_1", "tp"))
    return jax.shard_map(
        body,
        mesh=torus,
        in_specs=(
            P(SP, "tp"),
            P(SP, "tp"),
            P(SP, "tp"),
            P(SP, "tp"),
            P(SP, "tp"),
            P(None, "tp", SP),
            P(None, "tp", SP),
            P(None, "tp"),
            P(None, "tp"),
            P(None, "tp"),
            P(None, "tp"),
            P("tp"),
            P(None, "tp"),
            P(),
            P(SP, None),
            P(SP),
            P(SP, None),
            P(SP, None, "tp"),
            P(SP, None, "tp"),
            P(SP, "tp", None),
        ),
        out_specs=P(SP, "tp"),
        check_vma=False,
    )
```

profile of v0, /device:TPU:1, one launch (start us, length us, event | category | flops | bytes accessed | tf_op | source)
XLA Modules:
  0.0 280.2 jit_solution(5651927392031734438)
XLA Ops:
  0.0 0.9 constant_dynamic-update-slice_fusion.5
  0.9 0.8 constant_dynamic-update-slice_fusion.4
  2.4 3.9 %collective-permute-start = (bf16[2,384]{1,0:T(2,128)(2,1)S(1)}, bf16[2,384]{1,0:T(2,128)(2,1)S(1)}, u32[]{:S(2)}, u32[]{:S(2)}) collective-permute-start(bf16[2,384]{1,0:T(2,128)(2,1)S(1)} %get-tuple-element.47), channel_id=1, source_target_pairs={{0,16},{16,32},{32,48},{48,64},{64,80},{80,96},{96,112},{112,128},... | collective-permute-start | bytes 4616 | tf_op jit(solution)/shard_map/ppermute | solution.py:25
  6.3 1.3 collective-permute-start.1
  7.7 0.8 copy.71
  8.8 0.8 multiply_add_fusion
  15.4 10.4 %all-gather.6 = bf16[4,129,128]{2,1,0:T(8,128)(2,1)S(1)} all-gather(bf16[1,129,128]{2,1,0:T(8,128)(2,1)S(1)} %maximum_bitcast_fusion.2), channel_id=4, replica_groups=mesh['sp_0'=8,'sp_1'=4,'tp'=16] {'sp_1'}, dimensions={0}, use_global_device_ids=true | all-gather | bytes 165120 | tf_op jit(solution)/shard_map/all_gather | solution.py:48
  26.6 27.4 %all-gather.7 = bf16[8,129,128]{2,1,0:T(8,128)(2,1)S(1)} all-gather(bf16[1,129,128]{2,1,0:T(8,128)(2,1)S(1)} %maximum_bitcast_fusion.3), channel_id=5, replica_groups=mesh['sp_0'=8,'sp_1'=4,'tp'=16] {'sp_0'}, dimensions={0}, use_global_device_ids=true | all-gather | bytes 297216 | tf_op jit(solution)/shard_map/all_gather | solution.py:48
  54.2 9.1 %all-gather.4 = bf16[4,129,128]{2,1,0:T(8,128)(2,1)S(1)} all-gather(bf16[1,129,128]{2,1,0:T(8,128)(2,1)S(1)} %maximum_bitcast_fusion), channel_id=2, replica_groups=mesh['sp_0'=8,'sp_1'=4,'tp'=16] {'sp_1'}, dimensions={0}, use_global_device_ids=true | all-gather | bytes 165120 | tf_op jit(solution)/shard_map/all_gather | solution.py:48
  64.2 18.5 %all-gather.5 = bf16[8,129,128]{2,1,0:T(8,128)(2,1)S(1)} all-gather(bf16[1,129,128]{2,1,0:T(8,128)(2,1)S(1)} %maximum_bitcast_fusion.1), channel_id=3, replica_groups=mesh['sp_0'=8,'sp_1'=4,'tp'=16] {'sp_0'}, dimensions={0}, use_global_device_ids=true | all-gather | bytes 297216 | tf_op jit(solution)/shard_map/all_gather | solution.py:48
  84.8 37.9 %all_gather.38 = bf16[128,2048]{1,0:T(8,128)(2,1)S(1)} all-gather(bf16[128,128]{1,0:T(8,128)(2,1)S(1)} %multiply_convert_fusion.1), channel_id=1, replica_groups=mesh['sp_0'=8,'sp_1'=4,'tp'=16] {'tp'}, dimensions={1}, use_global_device_ids=true | all-gather | bytes 557056 | tf_op jit(solution)/shard_map/all_gather | solution.py:213
  123.0 16.4 %all_gather.39 = bf16[128,2048]{1,0:T(8,128)(2,1)S(1)} all-gather(bf16[128,128]{1,0:T(8,128)(2,1)S(1)} %fusion.6), channel_id=1, replica_groups=mesh['sp_0'=8,'sp_1'=4,'tp'=16] {'tp'}, dimensions={1}, use_global_device_ids=true | all-gather | bytes 557056 | tf_op jit(solution)/shard_map/all_gather | solution.py:220
  139.6 0.8 convolution_convert_fusion.1
  140.4 55.6 %all_to_all.15 = bf16[32,16,2048]{2,1,0:T(8,128)(2,1)S(1)} all-to-all(bf16[32,16,2048]{2,1,0:T(8,128)(2,1)S(1)} %bitcast.252), channel_id=1, replica_groups=mesh['sp_0'=8,'sp_1'=4,'tp'=16] {'sp_0','sp_1'}, dimensions={0} | all-to-all | bytes 4194304 | tf_op jit(solution)/shard_map/all_to_all | solution.py:244
  196.0 1.5 fusion.12
  197.5 5.0 %fusion = bf16[64,8,16,128]{3,1,2,0:T(8,128)(2,1)} fusion(bf16[1,256,2048]{2,1,0:T(8,128)(2,1)S(1)} %copy-done, bf16[512,2048]{1,0:T(8,128)(2,1)S(1)} %bitcast.256, bf16[1,2048,256]{2,1,0:T(8,128)(2,1)} %param.38, f32[512,256]{1,0:T(8,128)} %fusion.12), kind=kOutput, calls=%fused_computation.4 | convolution fusion | flops 1075576832 | bytes 6815744 | tf_op jit(solution)/shard_map/dot_general | solution.py:251
  202.6 2.2 copy.83
  204.8 1.9 copy.90
  206.7 6.9 %all-to-all-start.1 = ((bf16[16,32,16,128]{3,2,1,0:T(8,128)(2,1)}), bf16[16,32,16,128]{3,2,1,0:T(8,128)(2,1)S(1)}, u32[]{:S(2)}, u32[]{:S(2)}) async-start(bf16[16,32,16,128]{3,2,1,0:T(8,128)(2,1)} %bitcast.251), calls=%async_computation.1 | async-start | bytes 4194304 | tf_op jit(solution)/shard_map/all_to_all | solution.py:87
  214.2 48.5 %all-to-all-done.1 = bf16[16,32,16,128]{3,2,1,0:T(8,128)(2,1)S(1)} async-done(((bf16[16,32,16,128]{3,2,1,0:T(8,128)(2,1)}), bf16[16,32,16,128]{3,2,1,0:T(8,128)(2,1)S(1)}, u32[]{:S(2)}, u32[]{:S(2)}) %all-to-all-start.1) | async-done | bytes 2097184 | tf_op jit(solution)/shard_map/all_to_all | solution.py:87
  262.6 0.9 reduce_sum.69
  263.6 5.3 %all-to-all-start.2 = ((bf16[32,16,128]{2,1,0:T(8,128)(2,1)}), bf16[32,16,128]{2,1,0:T(8,128)(2,1)S(1)}, u32[]{:S(2)}, u32[]{:S(2)}) async-start(bf16[32,16,128]{2,1,0:T(8,128)(2,1)} %reduce_sum.69), calls=%async_computation.2 | async-start | bytes 262144 | tf_op jit(solution)/shard_map/all_to_all | solution.py:256
  268.9 9.4 %all-to-all-done.2 = bf16[32,16,128]{2,1,0:T(8,128)(2,1)S(1)} async-done(((bf16[32,16,128]{2,1,0:T(8,128)(2,1)}), bf16[32,16,128]{2,1,0:T(8,128)(2,1)S(1)}, u32[]{:S(2)}, u32[]{:S(2)}) %all-to-all-start.2) | async-done | bytes 131104 | tf_op jit(solution)/shard_map/all_to_all | solution.py:256
  278.3 0.9 gather_fusion
  (122 shorter events, 12.6 us)
Async XLA Ops:
  0.0 197.5 %copy-start = (bf16[1,256,2048]{2,1,0:T(8,128)(2,1)S(1)}, bf16[1,256,2048]{2,1,0:T(8,128)(2,1)}, u32[]{:S(2)}) copy-start(bf16[1,256,2048]{2,1,0:T(8,128)(2,1)} %param.39) | copy-start | bytes 3145732
  2.4 12.4 %collective-permute-start = (bf16[2,384]{1,0:T(2,128)(2,1)S(1)}, bf16[2,384]{1,0:T(2,128)(2,1)S(1)}, u32[]{:S(2)}, u32[]{:S(2)}) collective-permute-start(bf16[2,384]{1,0:T(2,128)(2,1)S(1)} %get-tuple-element.47), channel_id=1, source_target_pairs={{0,16},{16,32},{32,48},{48,64},{64,80},{80,96},{96,112},{112,128},... | collective-permute-start | bytes 4616 | tf_op jit(solution)/shard_map/ppermute | solution.py:25
  6.3 8.4 %collective-permute-start.1 = (bf16[2,384]{1,0:T(2,128)(2,1)S(1)}, bf16[2,384]{1,0:T(2,128)(2,1)S(1)}, u32[]{:S(2)}, u32[]{:S(2)}) collective-permute-start(bf16[2,384]{1,0:T(2,128)(2,1)S(1)} %get-tuple-element.48), channel_id=1, source_target_pairs={{16,0},{32,16},{48,32},{64,48},{80,64},{96,80},{112,96},{128,112},... | collective-permute-start | bytes 4616 | tf_op jit(solution)/shard_map/ppermute | solution.py:27
  82.7 1.9 copy-start.2
  82.7 2.0 copy-start.7
  82.7 40.0 %copy-start.1 = (bf16[2048,128]{1,0:T(8,128)(2,1)S(1)}, bf16[2048,128]{1,0:T(8,128)(2,1)}, u32[]{:S(2)}) copy-start(bf16[2048,128]{1,0:T(8,128)(2,1)} %param.32) | copy-start | bytes 1572868
  82.7 40.0 %copy-start.3 = (bf16[128,128]{1,0:T(8,128)(2,1)S(1)}, bf16[128,128]{1,0:T(8,128)(2,1)}, u32[]{:S(2)}) copy-start(bf16[128,128]{1,0:T(8,128)(2,1)} %param.20) | copy-start | bytes 98308
  83.9 55.7 %copy-start.5 = (f32[2048]{0:T(1024)S(1)}, f32[2048]{0:T(1024)}, u32[]{:S(2)}) copy-start(f32[2048]{0:T(1024)} %param.33) | copy-start | bytes 24580
  140.4 55.6 %copy-start.9 = (bf16[1,2048,256]{2,1,0:T(8,128)(2,1)S(1)}, bf16[1,2048,256]{2,1,0:T(8,128)(2,1)}, u32[]{:S(2)}) copy-start(bf16[1,2048,256]{2,1,0:T(8,128)(2,1)} %param.37) | copy-start | bytes 3145732
  206.7 6.9 %copy-start.4 = (s32[128,2]{0,1:T(2,128)S(1)}, s32[128,2]{0,1:T(2,128)}, u32[]{:S(2)}) copy-start(s32[128,2]{0,1:T(2,128)} %param.34) | copy-start | bytes 3076
  206.7 7.3 %copy-start.6 = (f32[128,2]{0,1:T(2,128)S(1)}, f32[128,2]{0,1:T(2,128)}, u32[]{:S(2)}) copy-start(f32[128,2]{0,1:T(2,128)} %param.36) | copy-start | bytes 3076
  206.7 7.4 %copy-start.8 = (f32[128]{0:T(128)S(1)}, f32[128]{0:T(128)}, u32[]{:S(2)}) copy-start(f32[128]{0:T(128)} %param.35) | copy-start | bytes 1540
  206.7 56.0 %all-to-all-start.1 = ((bf16[16,32,16,128]{3,2,1,0:T(8,128)(2,1)}), bf16[16,32,16,128]{3,2,1,0:T(8,128)(2,1)S(1)}, u32[]{:S(2)}, u32[]{:S(2)}) async-start(bf16[16,32,16,128]{3,2,1,0:T(8,128)(2,1)} %bitcast.251), calls=%async_computation.1 | async-start | bytes 4194304 | tf_op jit(solution)/shard_map/all_to_all | solution.py:87
  263.6 14.8 %all-to-all-start.2 = ((bf16[32,16,128]{2,1,0:T(8,128)(2,1)}), bf16[32,16,128]{2,1,0:T(8,128)(2,1)S(1)}, u32[]{:S(2)}, u32[]{:S(2)}) async-start(bf16[32,16,128]{2,1,0:T(8,128)(2,1)} %reduce_sum.69), calls=%async_computation.2 | async-start | bytes 262144 | tf_op jit(solution)/shard_map/all_to_all | solution.py:256
where the time goes:
time: 281 us; the launch traced here: 280 us
  blocking collectives  175 us (62%)
  waiting for transfers between devices  57.9 us (21%)
  starting transfers between devices  17.4 us (6%)
  local copies, waits for them, and re-layouts  13.4 us (5%)
  matrix products  9.61 us (3%)
  other arithmetic  6.01 us (2%)
    all_gather x4, blocking collectives, all_in_one(): both, at, found = (lax.all_gather(jnp.concatenate(lines), axis), 0, {})  65.3 us
    all_to_all x1, blocking collectives, body(): lax.all_to_all(outgoing, SP, split_axis=0, concat_axis=0, tiled=True)  55.6 us
    all_to_all x1, waiting for transfers between devices, sum_at_owner(): parts = lax.all_to_all(in_blocks(shard, dim, peers), axis, 0, 0, tiled=True)  48.5 us
    all_gather x1, blocking collectives, body(): lax.all_gather(mixed, 'tp', axis=1, tiled=True)  37.9 us
    all_gather x1, blocking collectives, body(): lax.all_gather(stream, 'tp', axis=1, tiled=True).astype(jnp.float32)  16.4 us
    all_to_all x1, waiting for transfers between devices, body(): lax.all_to_all(expert_cols, SP, split_axis=0, concat_axis=0, tiled=True)  9.43 us
    all_to_all x1, starting transfers between devices, sum_at_owner(): parts = lax.all_to_all(in_blocks(shard, dim, peers), axis, 0, 0, tiled=True)  6.91 us
    unnamed x30, local copies, waits for them, and re-layouts  6.06 us
  transfers between devices with their start and end apart: 4, of which 2 were waited for; matrix products, arithmetic and copies ran while one was open for 3% of the time, Pallas kernels for 0%

commit v1 on v0

--- a/solution.py
+++ b/solution.py
@@ -217,7 +217,9 @@
     stream = (skip_stream_entering.astype(jnp.float32) + projected).astype(jnp.bfloat16)
     stream_f = stream.astype(jnp.float32)
     col_count = skip_stream_entering.shape[1]
-    whole_rows = lax.all_gather(stream, "tp", axis=1, tiled=True).astype(jnp.float32)
+    whole_rows = jnp.concatenate(
+        lax.all_to_all(jnp.stack([stream] * lax.axis_size("tp")), "tp", 0, 0), axis=1
+    ).astype(jnp.float32)
     normal_rows = (
         whole_rows
         * lax.rsqrt(jnp.mean(whole_rows * whole_rows, axis=-1, keepdims=True) + stream_eps)

time: 281 us -> 282 us (level)
  waiting for transfers between devices: 57.9 us -> 73.5 us
  blocking collectives: 175 us -> 160 us
    all_gather x1 -> x0, blocking collectives: 16.4 us -> none  [body(): lax.all_gather(stream, 'tp', axis=1, tiled=True).astype(jnp.float32)]
    all_to_all x0 -> x1, waiting for transfers between devices: none -> 15.6 us  [body(): lax.all_to_all(jnp.stack([stream] * lax.axis_size('tp')), 'tp', 0, 0)]
    all_to_all x0 -> x1, starting transfers between devices: none -> 4.49 us  [body(): lax.all_to_all(jnp.stack([stream] * lax.axis_size('tp')), 'tp', 0, 0)]
    all_to_all x1, starting transfers between devices: 6.91 us -> 4.03 us  [sum_at_owner(): parts = lax.all_to_all(in_blocks(shard, dim, peers), axis, 0, 0, tiled=True)]
  transfers between devices with their start and end apart: 4 -> 5, of which waited for: 2 -> 3; matrix products, arithmetic and copies ran while one was open for 3% -> 2% of each run, Pallas kernels for 0% -> 0%
where the time goes in v1:
time: 282 us
  blocking collectives  160 us (57%)
  waiting for transfers between devices  73.5 us (26%)
  starting transfers between devices  18.9 us (7%)
  local copies, waits for them, and re-layouts  13.7 us (5%)
  matrix products  9.54 us (3%)
  other arithmetic  5.76 us (2%)
    all_gather x4, blocking collectives, all_in_one(): both, at, found = (lax.all_gather(jnp.concatenate(lines), axis), 0, {})  65.6 us
    all_to_all x1, blocking collectives, body(): lax.all_to_all(outgoing, SP, split_axis=0, concat_axis=0, tiled=True)  56.4 us
    all_to_all x1, waiting for transfers between devices, sum_at_owner(): parts = lax.all_to_all(in_blocks(shard, dim, peers), axis, 0, 0, tiled=True)  48.5 us
    all_gather x1, blocking collectives, body(): lax.all_gather(mixed, 'tp', axis=1, tiled=True)  37.5 us
    all_to_all x1, waiting for transfers between devices, body(): lax.all_to_all(jnp.stack([stream] * lax.axis_size('tp')), 'tp', 0, 0)  15.6 us
    all_to_all x1, waiting for transfers between devices, body(): lax.all_to_all(expert_cols, SP, split_axis=0, concat_axis=0, tiled=True)  9.43 us
  transfers between devices with their start and end apart: 5, of which 3 were waited for; matrix products, arithmetic and copies ran while one was open for 2% of the time, Pallas kernels for 0%

profile of v1, /device:TPU:1, one launch (start us, length us, event | category | flops | bytes accessed | tf_op | source)
XLA Modules:
  0.0 281.6 jit_solution(8827319356396818228)
XLA Ops:
  0.0 0.9 constant_dynamic-update-slice_fusion.5
  0.9 0.8 constant_dynamic-update-slice_fusion.4
  2.4 3.9 %collective-permute-start = (bf16[2,384]{1,0:T(2,128)(2,1)S(1)}, bf16[2,384]{1,0:T(2,128)(2,1)S(1)}, u32[]{:S(2)}, u32[]{:S(2)}) collective-permute-start(bf16[2,384]{1,0:T(2,128)(2,1)S(1)} %get-tuple-element.47), channel_id=1, source_target_pairs={{0,16},{16,32},{32,48},{48,64},{64,80},{80,96},{96,112},{112,128},... | collective-permute-start | bytes 4616 | tf_op jit(solution)/shard_map/ppermute | solution.py:25
  6.3 1.3 collective-permute-start.1
  7.7 0.8 multiply_add_fusion
  12.4 10.7 %all-gather.6 = bf16[4,129,128]{2,1,0:T(8,128)(2,1)S(1)} all-gather(bf16[1,129,128]{2,1,0:T(8,128)(2,1)S(1)} %maximum_bitcast_fusion.2), channel_id=4, replica_groups=mesh['sp_0'=8,'sp_1'=4,'tp'=16] {'sp_1'}, dimensions={0}, use_global_device_ids=true | all-gather | bytes 165120 | tf_op jit(solution)/shard_map/all_gather | solution.py:48
  23.9 27.0 %all-gather.7 = bf16[8,129,128]{2,1,0:T(8,128)(2,1)S(1)} all-gather(bf16[1,129,128]{2,1,0:T(8,128)(2,1)S(1)} %maximum_bitcast_fusion.3), channel_id=5, replica_groups=mesh['sp_0'=8,'sp_1'=4,'tp'=16] {'sp_0'}, dimensions={0}, use_global_device_ids=true | all-gather | bytes 297216 | tf_op jit(solution)/shard_map/all_gather | solution.py:48
  51.2 9.1 %all-gather.4 = bf16[4,129,128]{2,1,0:T(8,128)(2,1)S(1)} all-gather(bf16[1,129,128]{2,1,0:T(8,128)(2,1)S(1)} %maximum_bitcast_fusion), channel_id=2, replica_groups=mesh['sp_0'=8,'sp_1'=4,'tp'=16] {'sp_1'}, dimensions={0}, use_global_device_ids=true | all-gather | bytes 165120 | tf_op jit(solution)/shard_map/all_gather | solution.py:48
  61.2 18.8 %all-gather.5 = bf16[8,129,128]{2,1,0:T(8,128)(2,1)S(1)} all-gather(bf16[1,129,128]{2,1,0:T(8,128)(2,1)S(1)} %maximum_bitcast_fusion.1), channel_id=3, replica_groups=mesh['sp_0'=8,'sp_1'=4,'tp'=16] {'sp_0'}, dimensions={0}, use_global_device_ids=true | all-gather | bytes 297216 | tf_op jit(solution)/shard_map/all_gather | solution.py:48
  82.1 37.5 %all_gather.35 = bf16[128,2048]{1,0:T(8,128)(2,1)S(1)} all-gather(bf16[128,128]{1,0:T(8,128)(2,1)S(1)} %multiply_convert_fusion.1), channel_id=1, replica_groups=mesh['sp_0'=8,'sp_1'=4,'tp'=16] {'tp'}, dimensions={1}, use_global_device_ids=true | all-gather | bytes 557056 | tf_op jit(solution)/shard_map/all_gather | solution.py:213
  120.1 0.9 stack.5
  121.0 4.5 %all-to-all-start = ((bf16[16,128,128]{1,2,0:T(8,128)(2,1)}), bf16[16,128,128]{1,2,0:T(8,128)(2,1)S(1)}, u32[]{:S(2)}, u32[]{:S(2)}) async-start(bf16[16,128,128]{1,2,0:T(8,128)(2,1)} %stack.5), calls=%async_computation | async-start | bytes 1048576 | tf_op jit(solution)/shard_map/all_to_all | solution.py:221
  127.1 15.6 %all-to-all-done = bf16[16,128,128]{1,2,0:T(8,128)(2,1)S(1)} async-done(((bf16[16,128,128]{1,2,0:T(8,128)(2,1)}), bf16[16,128,128]{1,2,0:T(8,128)(2,1)S(1)}, u32[]{:S(2)}, u32[]{:S(2)}) %all-to-all-start) | async-done | bytes 524320 | tf_op jit(solution)/shard_map/all_to_all | solution.py:221
  144.0 56.4 %all_to_all.20 = bf16[32,16,2048]{2,1,0:T(8,128)(2,1)S(1)} all-to-all(bf16[32,16,2048]{2,1,0:T(8,128)(2,1)S(1)} %bitcast.261), channel_id=1, replica_groups=mesh['sp_0'=8,'sp_1'=4,'tp'=16] {'sp_0','sp_1'}, dimensions={0} | all-to-all | bytes 4194304 | tf_op jit(solution)/shard_map/all_to_all | solution.py:246
  200.4 1.5 fusion.11
  201.9 5.0 %fusion = bf16[64,8,16,128]{3,1,2,0:T(8,128)(2,1)} fusion(bf16[1,256,2048]{2,1,0:T(8,128)(2,1)S(1)} %copy-done, bf16[512,2048]{1,0:T(8,128)(2,1)S(1)} %bitcast.265, bf16[1,2048,256]{2,1,0:T(8,128)(2,1)} %param.38, f32[512,256]{1,0:T(8,128)} %fusion.11), kind=kOutput, calls=%fused_computation.4 | convolution fusion | flops 1075576832 | bytes 6815744 | tf_op jit(solution)/shard_map/dot_general | solution.py:253
  206.9 2.2 copy.88
  209.2 1.9 copy.95
  211.1 4.0 %all-to-all-start.2 = ((bf16[16,32,16,128]{3,2,1,0:T(8,128)(2,1)}), bf16[16,32,16,128]{3,2,1,0:T(8,128)(2,1)S(1)}, u32[]{:S(2)}, u32[]{:S(2)}) async-start(bf16[16,32,16,128]{3,2,1,0:T(8,128)(2,1)} %bitcast.260), calls=%async_computation.2 | async-start | bytes 4194304 | tf_op jit(solution)/shard_map/all_to_all | solution.py:87
  215.7 48.5 %all-to-all-done.2 = bf16[16,32,16,128]{3,2,1,0:T(8,128)(2,1)S(1)} async-done(((bf16[16,32,16,128]{3,2,1,0:T(8,128)(2,1)}), bf16[16,32,16,128]{3,2,1,0:T(8,128)(2,1)S(1)}, u32[]{:S(2)}, u32[]{:S(2)}) %all-to-all-start.2) | async-done | bytes 2097184 | tf_op jit(solution)/shard_map/all_to_all | solution.py:87
  264.2 0.9 reduce_sum.69
  265.1 5.2 %all-to-all-start.3 = ((bf16[32,16,128]{2,1,0:T(8,128)(2,1)}), bf16[32,16,128]{2,1,0:T(8,128)(2,1)S(1)}, u32[]{:S(2)}, u32[]{:S(2)}) async-start(bf16[32,16,128]{2,1,0:T(8,128)(2,1)} %reduce_sum.69), calls=%async_computation.3 | async-start | bytes 262144 | tf_op jit(solution)/shard_map/all_to_all | solution.py:258
  270.4 9.4 %all-to-all-done.3 = bf16[32,16,128]{2,1,0:T(8,128)(2,1)S(1)} async-done(((bf16[32,16,128]{2,1,0:T(8,128)(2,1)}), bf16[32,16,128]{2,1,0:T(8,128)(2,1)S(1)}, u32[]{:S(2)}, u32[]{:S(2)}) %all-to-all-start.3) | async-done | bytes 131104 | tf_op jit(solution)/shard_map/all_to_all | solution.py:258
  279.8 0.9 gather_fusion
  (126 shorter events, 13.3 us)
Async XLA Ops:
  0.0 201.9 %copy-start = (bf16[1,256,2048]{2,1,0:T(8,128)(2,1)S(1)}, bf16[1,256,2048]{2,1,0:T(8,128)(2,1)}, u32[]{:S(2)}) copy-start(bf16[1,256,2048]{2,1,0:T(8,128)(2,1)} %param.39) | copy-start | bytes 3145732
  2.4 9.4 %collective-permute-start = (bf16[2,384]{1,0:T(2,128)(2,1)S(1)}, bf16[2,384]{1,0:T(2,128)(2,1)S(1)}, u32[]{:S(2)}, u32[]{:S(2)}) collective-permute-start(bf16[2,384]{1,0:T(2,128)(2,1)S(1)} %get-tuple-element.47), channel_id=1, source_target_pairs={{0,16},{16,32},{32,48},{48,64},{64,80},{80,96},{96,112},{112,128},... | collective-permute-start | bytes 4616 | tf_op jit(solution)/shard_map/ppermute | solution.py:25
  6.3 5.5 %collective-permute-start.1 = (bf16[2,384]{1,0:T(2,128)(2,1)S(1)}, bf16[2,384]{1,0:T(2,128)(2,1)S(1)}, u32[]{:S(2)}, u32[]{:S(2)}) collective-permute-start(bf16[2,384]{1,0:T(2,128)(2,1)S(1)} %get-tuple-element.48), channel_id=1, source_target_pairs={{16,0},{32,16},{48,32},{64,48},{80,64},{96,80},{112,96},{128,112},... | collective-permute-start | bytes 4616 | tf_op jit(solution)/shard_map/ppermute | solution.py:27
  80.0 1.9 copy-start.2
  80.0 2.0 copy-start.7
  80.0 39.6 %copy-start.1 = (bf16[2048,128]{1,0:T(8,128)(2,1)S(1)}, bf16[2048,128]{1,0:T(8,128)(2,1)}, u32[]{:S(2)}) copy-start(bf16[2048,128]{1,0:T(8,128)(2,1)} %param.32) | copy-start | bytes 1572868
  80.0 39.6 %copy-start.3 = (bf16[128,128]{1,0:T(8,128)(2,1)S(1)}, bf16[128,128]{1,0:T(8,128)(2,1)}, u32[]{:S(2)}) copy-start(bf16[128,128]{1,0:T(8,128)(2,1)} %param.20) | copy-start | bytes 98308
  81.2 44.2 %copy-start.4 = (s32[128,2]{0,1:T(2,128)S(1)}, s32[128,2]{0,1:T(2,128)}, u32[]{:S(2)}) copy-start(s32[128,2]{0,1:T(2,128)} %param.34) | copy-start | bytes 3076
  119.6 23.3 %copy-start.5 = (f32[2048]{0:T(1024)S(1)}, f32[2048]{0:T(1024)}, u32[]{:S(2)}) copy-start(f32[2048]{0:T(1024)} %param.33) | copy-start | bytes 24580
  121.0 21.7 %all-to-all-start = ((bf16[16,128,128]{1,2,0:T(8,128)(2,1)}), bf16[16,128,128]{1,2,0:T(8,128)(2,1)S(1)}, u32[]{:S(2)}, u32[]{:S(2)}) async-start(bf16[16,128,128]{1,2,0:T(8,128)(2,1)} %stack.5), calls=%async_computation | async-start | bytes 1048576 | tf_op jit(solution)/shard_map/all_to_all | solution.py:221
  144.0 56.4 %copy-start.9 = (bf16[1,2048,256]{2,1,0:T(8,128)(2,1)S(1)}, bf16[1,2048,256]{2,1,0:T(8,128)(2,1)}, u32[]{:S(2)}) copy-start(bf16[1,2048,256]{2,1,0:T(8,128)(2,1)} %param.37) | copy-start | bytes 3145732
  211.1 4.4 %copy-start.6 = (f32[128,2]{0,1:T(2,128)S(1)}, f32[128,2]{0,1:T(2,128)}, u32[]{:S(2)}) copy-start(f32[128,2]{0,1:T(2,128)} %param.36) | copy-start | bytes 3076
  211.1 4.5 %copy-start.8 = (f32[128]{0:T(128)S(1)}, f32[128]{0:T(128)}, u32[]{:S(2)}) copy-start(f32[128]{0:T(128)} %param.35) | copy-start | bytes 1540
  211.1 53.1 %all-to-all-start.2 = ((bf16[16,32,16,128]{3,2,1,0:T(8,128)(2,1)}), bf16[16,32,16,128]{3,2,1,0:T(8,128)(2,1)S(1)}, u32[]{:S(2)}, u32[]{:S(2)}) async-start(bf16[16,32,16,128]{3,2,1,0:T(8,128)(2,1)} %bitcast.260), calls=%async_computation.2 | async-start | bytes 4194304 | tf_op jit(solution)/shard_map/all_to_all | solution.py:87
  265.1 14.7 %all-to-all-start.3 = ((bf16[32,16,128]{2,1,0:T(8,128)(2,1)}), bf16[32,16,128]{2,1,0:T(8,128)(2,1)S(1)}, u32[]{:S(2)}, u32[]{:S(2)}) async-start(bf16[32,16,128]{2,1,0:T(8,128)(2,1)} %reduce_sum.69), calls=%async_computation.3 | async-start | bytes 262144 | tf_op jit(solution)/shard_map/all_to_all | solution.py:258
